TPU v7x, 32 devices: a whole 2x2x4 slice. The times are simulated.
32 devices in a mesh: ra: 4 (over y, x), cb: 8 (over z, core).
Axes of the slice: x: 2, y: 2, z: 4, core: 2. Of those that a mesh axis runs over, the one named last changes fastest.
Arguments:
- tokens: bfloat16 [2048, 2048], P('cb', 'ra'), may hold values from -40 to 40
- gain_first: float32 [2048], replicated, may hold values from 0.1 to 1.9
- gate_first: float32 [2048, 5632], P('cb', 'ra'), may hold values from -0.125 to 0.125
- gate_first_scale: float32 [5632], P('ra'), may hold values from 0.5 to 2
- up_first: float32 [2048, 5632], P('cb', 'ra'), may hold values from -0.125 to 0.125
- up_first_scale: float32 [5632], P('ra'), may hold values from 0.5 to 2
- down_first: float32 [5632, 2048], P('ra', 'cb'), may hold values from -0.078125 to 0.078125
- down_first_scale: float32 [2048], replicated, may hold values from 0.5 to 2
- gain_second: float32 [2048], replicated, may hold values from 0.1 to 1.9
- gate_second: float32 [2048, 5632], P('cb', 'ra'), may hold values from -0.125 to 0.125
- gate_second_scale: float32 [5632], P('ra'), may hold values from 0.5 to 2
- up_second: float32 [2048, 5632], P('cb', 'ra'), may hold values from -0.125 to 0.125
- up_second_scale: float32 [5632], P('ra'), may hold values from 0.5 to 2
- down_second: float32 [5632, 2048], P('ra', 'cb'), may hold values from -0.078125 to 0.078125
- down_second_scale: float32 [2048], replicated, may hold values from 0.5 to 2
- gain_last: float32 [2048], replicated, may hold values from 0.1 to 1.9
Outputs:
- mixed: bfloat16 [2048, 2048], P('cb', 'ra')
All inputs are finite; a program needn't handle non-finite values.
Results may differ from a plain program's by a relative error of at most 0.025.
Values may be sent and summed in bfloat16 or wider, within the bound.
A program may use at most 64 MiB of HBM per device.

v0:
```python
import jax
import jax.numpy as jnp
from jax import lax
from jax.sharding import PartitionSpec as P

D = 2048


def own_slice(vector, width):
    return lax.dynamic_slice_in_dim(vector, lax.axis_index("ra") * width, width, 0)


def full_norm(values, gain):
    meansq = jnp.mean(values * values, axis=1, keepdims=True)
    return (values * lax.rsqrt(meansq + 1e-06) * gain).astype(jnp.bfloat16)


def expand(normed, w_gate, s_gate, w_up, s_up, w_down):
    gate = jnp.dot(
        normed,
        lax.all_gather(w_gate.astype(jnp.bfloat16), "cb", axis=0, tiled=True),
        preferred_element_type=jnp.float32,
    )
    upper = jnp.dot(
        normed,
        lax.all_gather(w_up.astype(jnp.bfloat16), "cb", axis=0, tiled=True),
        preferred_element_type=jnp.float32,
    )
    hidden = (jax.nn.silu(gate * s_gate) * (upper * s_up)).astype(jnp.bfloat16)
    return jnp.dot(
        hidden,
        lax.all_gather(w_down.astype(jnp.bfloat16), "cb", axis=1, tiled=True),
        preferred_element_type=jnp.float32,
    )


def reduce_share(partial_value):
    return lax.psum_scatter(
        partial_value.astype(jnp.bfloat16), "ra", scatter_dimension=1, tiled=True
    ).astype(jnp.float32)


def shards(
    tokens,
    gain_first,
    gate_first,
    gate_first_scale,
    up_first,
    up_first_scale,
    down_first,
    down_first_scale,
    gain_second,
    gate_second,
    gate_second_scale,
    up_second,
    up_second_scale,
    down_second,
    down_second_scale,
    gain_last,
):
    width = tokens.shape[1]
    whole_in = lax.all_gather(tokens, "ra", axis=1, tiled=True).astype(jnp.float32)
    normed = full_norm(whole_in, gain_first)
    partial_value = expand(
        normed, gate_first, gate_first_scale, up_first, up_first_scale, down_first
    )
    summed = lax.psum(partial_value.astype(jnp.bfloat16), "ra").astype(jnp.float32)
    first = 0.1 * whole_in + 0.5 * summed * down_first_scale
    first_share = own_slice(first.T, width).T
    normed_next = full_norm(first, gain_second)
    partial_next = expand(
        normed_next, gate_second, gate_second_scale, up_second, up_second_scale, down_second
    )
    second = 0.1 * first_share + 0.5 * reduce_share(partial_next) * own_slice(
        down_second_scale, width
    )
    closing = lax.psum(jnp.sum(second * second, axis=1), "ra")
    return (second * lax.rsqrt(closing / D + 1e-06)[:, None] * own_slice(gain_last, width)).astype(
        jnp.bfloat16
    )


def solution(mesh):
    placed = (
        P("cb", "ra"),
        P(),
        P("cb", "ra"),
        P("ra"),
        P("cb", "ra"),
        P("ra"),
        P("ra", "cb"),
        P(),
        P(),
        P("cb", "ra"),
        P("ra"),
        P("cb", "ra"),
        P("ra"),
        P("ra", "cb"),
        P(),
        P(),
    )
    return jax.shard_map(
        shards, mesh=mesh, in_specs=placed, out_specs=P("cb", "ra"), check_vma=False
    )
```

profile of v0, /device:TPU:0, one launch (start us, length us, event | category | flops | bytes accessed | tf_op | source)
XLA Modules:
  0.0 519.8 jit_solution(4151006821020367935)
XLA Ops:
  6.5 0.7 all-gather.8.cloned.1.call-update
  7.3 2.3 convert_element_type.50
  9.6 0.0 all-gather.12.cloned.1.call-start
  9.7 0.9 convert_element_type.51
  10.7 0.0 all-gather.14.cloned.1.call-start
  10.7 0.5 copy-done.2
  11.2 0.9 convert_element_type.53
  12.3 26.0 %all-gather.8.cloned.1.call-done = bf16[256,2048]{1,0:T(8,128)(2,1)} async-done(((bf16[256,512]{1,0:T(8,128)(2,1)}), bf16[256,2048]{1,0:T(8,128)(2,1)}) %all-gather.8.cloned.1.call-update) | async-done | bytes 1048592 | tf_op jit(solution)/shard_map/all_gather | solution.py:62
  38.3 1.5 fusion.5
  39.8 60.5 %all-gather.10.cloned.1.call-done = bf16[2048,1408]{1,0:T(8,128)(2,1)} async-done(((bf16[256,1408]{1,0:T(8,128)(2,1)}), bf16[2048,1408]{1,0:T(8,128)(2,1)}) %all-gather.10.cloned.1.call-update) | async-done | bytes 5767184 | tf_op jit(solution)/shard_map/all_gather | solution.py:21
  100.3 6.0 %convolution_multiply_fusion.3 = f32[256,1408]{1,0:T(8,128)} fusion(bf16[2048,1408]{1,0:T(8,128)(2,1)} %all-gather.10.cloned.1.call-done, f32[1408]{0:T(1024)S(1)} %copy-done.6, bf16[256,2048]{1,0:T(8,128)(2,1)} %all-gather.8.cloned.1.call-done, f32[2048]{0:T(1024)S(1)} %copy-done.7, f32[256]{0:T(256)S(1)} %add_rsqrt_fusion.2), kind=kOutput, calls=%fused_computation.8 | convolution fusion | flops 1478852608 | bytes 8272384 | tf_op jit(solution)/shard_map/dot_general | solution.py:19
  106.3 54.8 %all-gather.12.cloned.1.call-done = bf16[2048,1408]{1,0:T(8,128)(2,1)} async-done(((bf16[256,1408]{1,0:T(8,128)(2,1)}), bf16[2048,1408]{1,0:T(8,128)(2,1)}) %all-gather.12.cloned.1.call-update) | async-done | bytes 5767184 | tf_op jit(solution)/shard_map/all_gather | solution.py:26
  161.0 61.0 %all-gather.14.cloned.1.call-done = bf16[1408,2048]{1,0:T(8,128)(2,1)} async-done(((bf16[1408,256]{1,0:T(8,128)(2,1)}), bf16[1408,2048]{1,0:T(8,128)(2,1)}) %all-gather.14.cloned.1.call-update) | async-done | bytes 5767184 | tf_op jit(solution)/shard_map/all_gather | solution.py:32
  222.0 9.3 %convolution_convert_fusion.1 = bf16[256,2048]{1,0:T(8,128)(2,1)} fusion(bf16[1408,2048]{1,0:T(8,128)(2,1)} %all-gather.14.cloned.1.call-done, bf16[2048,1408]{1,0:T(8,128)(2,1)} %all-gather.12.cloned.1.call-done, f32[256,1408]{1,0:T(8,128)} %convolution_multiply_fusion.3, f32[1408]{0:T(1024)S(1)} %copy-done.8, bf16[256,2048]{1,0:T(8,128)(2,1)S(1)} %copy-done, ...), kind=kOutput, calls=%fused_computation.12 | convolution fusion | flops 2957934592 | bytes 15088128 | tf_op jit(solution)/shard_map/dot_general | solution.py:30
  231.3 0.0 all-gather.16.cloned.1.call-start
  231.4 0.9 convert_element_type.57
  232.4 2.4 convert_element_type.58
  234.9 0.9 convert_element_type.60
  235.8 0.0 reduce-scatter.2.cloned.1.call-start
  235.9 46.2 %all-reduce.2.cloned.1.call-done = bf16[256,2048]{1,0:T(8,128)(2,1)} async-done(((bf16[256,2048]{1,0:T(8,128)(2,1)}), bf16[256,2048]{1,0:T(8,128)(2,1)}) %all-reduce.2.cloned.1.call-update) | async-done | bytes 1048592 | tf_op jit(solution)/shard_map/psum | solution.py:67
  282.1 1.8 multiply_reduce_fusion
  283.9 60.1 %all-gather.16.cloned.1.call-done = bf16[2048,1408]{1,0:T(8,128)(2,1)} async-done(((bf16[256,1408]{1,0:T(8,128)(2,1)}), bf16[2048,1408]{1,0:T(8,128)(2,1)}) %all-gather.16.cloned.1.call-update) | async-done | bytes 5767184 | tf_op jit(solution)/shard_map/all_gather | solution.py:21
  344.0 5.6 %convolution_multiply_fusion.1 = f32[256,1408]{1,0:T(8,128)} fusion(bf16[2048,1408]{1,0:T(8,128)(2,1)} %all-gather.16.cloned.1.call-done, f32[1408]{0:T(1024)S(1)} %copy-done.9, f32[256,2048]{1,0:T(8,128)S(1)} %get-tuple-element.6, f32[2048]{0:T(1024)S(1)} %copy-done.10, f32[256]{0:T(256)S(1)} %add_rsqrt_fusion.1), kind=kOutput, calls=%fused_computation.5 | convolution fusion | flops 1478328320 | bytes 9320960 | tf_op jit(solution)/shard_map/dot_general | solution.py:19
  349.6 55.1 %all-gather.18.cloned.1.call-done = bf16[2048,1408]{1,0:T(8,128)(2,1)} async-done(((bf16[256,1408]{1,0:T(8,128)(2,1)}), bf16[2048,1408]{1,0:T(8,128)(2,1)}) %all-gather.18.cloned.1.call-update) | async-done | bytes 5767184 | tf_op jit(solution)/shard_map/all_gather | solution.py:26
  404.7 61.1 %all-gather.20.cloned.1.call-done = bf16[1408,2048]{1,0:T(8,128)(2,1)} async-done(((bf16[1408,256]{1,0:T(8,128)(2,1)}), bf16[1408,2048]{1,0:T(8,128)(2,1)}) %all-gather.20.cloned.1.call-update) | async-done | bytes 5767184 | tf_op jit(solution)/shard_map/all_gather | solution.py:32
  465.8 9.3 %convolution_convert_fusion = bf16[256,2048]{1,0:T(8,128)(2,1)} fusion(bf16[1408,2048]{1,0:T(8,128)(2,1)} %all-gather.20.cloned.1.call-done, bf16[2048,1408]{1,0:T(8,128)(2,1)} %all-gather.18.cloned.1.call-done, f32[256,1408]{1,0:T(8,128)} %convolution_multiply_fusion.1, f32[1408]{0:T(1024)S(1)} %copy-done.11, f32[256,2048]{1,0:T(8,128)S(1)} %get-tuple-element.6, ...), kind=kOutput, calls=%fused_computation.11 | convolution fusion | flops 2957410304 | bytes 16136704 | tf_op jit(solution)/shard_map/dot_general | solution.py:30
  475.1 0.8 dynamic_slice.8
  475.9 0.8 dynamic-slice_multiply_fusion
  476.6 24.8 %reduce-scatter.2.cloned.1.call-done = bf16[256,512]{1,0:T(8,128)(2,1)} async-done(((bf16[256,2048]{1,0:T(8,128)(2,1)}), bf16[256,512]{1,0:T(8,128)(2,1)}) %reduce-scatter.2.cloned.1.call-update) | async-done | bytes 262160 | tf_op jit(solution)/shard_map/reduce_scatter | solution.py:38
  501.4 1.1 multiply_reduce_fusion.1
  502.5 8.9 %psum.15 = f32[256]{0:T(256)S(1)} all-reduce(f32[256]{0:T(256)S(1)} %multiply_reduce_fusion.1), channel_id=1, replica_groups=mesh['ra'=4,'cb'=8] {'ra'}, use_global_device_ids=true, to_apply=%region_5.6 | all-reduce | flops 256 | bytes 2048 | tf_op jit(solution)/shard_map/psum | solution.py:77
  511.5 1.8 multiply_convert_fusion.1
  (40 shorter events, 0.4 us)
Async XLA Ops:
  6.5 3.2 copy-start.1
  6.5 31.7 %all-gather.8.cloned.1.call-start = ((), (), s32[]{:S(2)}) async-start(), calls=%async_computation.1 | async-start | bytes 1310720 | tf_op jit(solution)/shard_map/all_gather | solution.py:62
  7.3 93.0 %all-gather.10.cloned.1.call-start = ((), (), s32[]{:S(2)}) async-start(), calls=%async_computation.2 | async-start | bytes 6488064 | tf_op jit(solution)/shard_map/all_gather | solution.py:21
  9.6 1.6 copy-start.2
  9.6 151.4 %all-gather.12.cloned.1.call-start = ((), (), s32[]{:S(2)}) async-start(), calls=%async_computation.3 | async-start | bytes 6488064 | tf_op jit(solution)/shard_map/all_gather | solution.py:26
  10.7 89.6 %copy-start.6 = (f32[1408]{0:T(1024)S(1)}, f32[1408]{0:T(1024)}, u32[]{:S(2)}) copy-start(f32[1408]{0:T(1024)} %param.19) | copy-start | bytes 16900
  10.7 89.6 %copy-start.7 = (f32[2048]{0:T(1024)S(1)}, f32[2048]{0:T(1024)}, u32[]{:S(2)}) copy-start(f32[2048]{0:T(1024)} %param.17) | copy-start | bytes 24580
  10.7 211.3 %all-gather.14.cloned.1.call-start = ((), (), s32[]{:S(2)}) async-start(), calls=%async_computation.4 | async-start | bytes 6488064 | tf_op jit(solution)/shard_map/all_gather | solution.py:32
  12.2 269.9 %all-reduce.2.cloned.1.call-start = ((), (), s32[]{:S(2)}) async-start(), calls=%async_computation.5 | async-start | bytes 2097152 | tf_op jit(solution)/shard_map/psum | solution.py:67
  39.8 182.2 %copy-start = (bf16[256,2048]{1,0:T(8,128)(2,1)S(1)}, bf16[256,2048]{1,0:T(8,128)(2,1)}, u32[]{:S(2)}) copy-start(bf16[256,2048]{1,0:T(8,128)(2,1)} %all-gather.8.cloned.1.call-done) | copy-start | bytes 3145732
  39.8 182.2 %copy-start.8 = (f32[1408]{0:T(1024)S(1)}, f32[1408]{0:T(1024)}, u32[]{:S(2)}) copy-start(f32[1408]{0:T(1024)} %param.21) | copy-start | bytes 16900
  106.3 125.1 %copy-start.3 = (f32[256,1408]{1,0:T(8,128)S(1)}, f32[256,1408]{1,0:T(8,128)}, u32[]{:S(2)}) copy-start(f32[256,1408]{1,0:T(8,128)} %param.25) | copy-start | bytes 4325380
  231.3 112.7 %all-gather.16.cloned.1.call-start = ((), (), s32[]{:S(2)}) async-start(), calls=%async_computation.6 | async-start | bytes 6488064 | tf_op jit(solution)/shard_map/all_gather | solution.py:21
  232.3 2.6 copy-start.4
  232.3 172.4 %all-gather.18.cloned.1.call-start = ((), (), s32[]{:S(2)}) async-start(), calls=%async_computation.7 | async-start | bytes 6488064 | tf_op jit(solution)/shard_map/all_gather | solution.py:26
  234.8 1.1 copy-start.5
  234.8 231.0 %all-gather.20.cloned.1.call-start = ((), (), s32[]{:S(2)}) async-start(), calls=%async_computation.8 | async-start | bytes 6488064 | tf_op jit(solution)/shard_map/all_gather | solution.py:32
  235.8 265.6 %reduce-scatter.2.cloned.1.call-start = ((), (), s32[]{:S(2)}) async-start(), calls=%async_computation.9 | async-start | bytes 1310720 | tf_op jit(solution)/shard_map/reduce_scatter | solution.py:38
  235.9 108.1 %copy-start.9 = (f32[1408]{0:T(1024)S(1)}, f32[1408]{0:T(1024)}, u32[]{:S(2)}) copy-start(f32[1408]{0:T(1024)} %param.26) | copy-start | bytes 16900
  235.9 108.1 %copy-start.10 = (f32[2048]{0:T(1024)S(1)}, f32[2048]{0:T(1024)}, u32[]{:S(2)}) copy-start(f32[2048]{0:T(1024)} %param.24) | copy-start | bytes 24580
  344.0 121.8 %copy-start.11 = (f32[1408]{0:T(1024)S(1)}, f32[1408]{0:T(1024)}, u32[]{:S(2)}) copy-start(f32[1408]{0:T(1024)} %param.28) | copy-start | bytes 16900
Sparse Core Ops, SparseCore 0:
  9.2 29.0 all-gather.7
  39.9 60.3 all-gather.9
  102.0 59.0 all-gather.11
  162.5 59.4 all-gather.13
  231.4 50.6 all-reduce.1
  283.6 60.3 all-gather.15
  345.6 59.0 all-gather.17
  406.3 59.4 all-gather.19
  475.2 26.1 reduce-scatter.1
where the time goes:
time: 520 us
  waiting for transfers between devices  450 us (87%)
  matrix products  30.1 us (6%)
  other arithmetic  15.5 us (3%)
  between operations  13.3 us (3%)
  blocking collectives  8.93 us (2%)
    all_gather x2, waiting for transfers between devices, expand(): lax.all_gather(w_down.astype(jnp.bfloat16), 'cb', axis=1, tiled=True)  122 us
    all_gather x2, waiting for transfers between devices, expand(): lax.all_gather(w_gate.astype(jnp.bfloat16), 'cb', axis=0, tiled=True)  121 us
    all_gather x2, waiting for transfers between devices, expand(): lax.all_gather(w_up.astype(jnp.bfloat16), 'cb', axis=0, tiled=True)  110 us
    psum x1, waiting for transfers between devices, shards(): lax.psum(partial_value.astype(jnp.bfloat16), 'ra').astype(jnp.float32)  46.2 us
    all_gather x1, waiting for transfers between devices, shards(): lax.all_gather(tokens, 'ra', axis=1, tiled=True).astype(jnp.float32)  26 us
    reduce_scatter x1, waiting for transfers between devices, reduce_share(): lax.psum_scatter(partial_value.astype(jnp.bfloat16), 'ra', scatter_dimens...  24.8 us
    dot_general x2, matrix products, expand(): jnp.dot(hidden, lax.all_gather(w_down.astype(jnp.bfloat16), 'cb', axis=1,...  18.5 us
    dot_general x2, matrix products, expand(): jnp.dot(normed, lax.all_gather(w_gate.astype(jnp.bfloat16), 'cb', axis=0,...  11.6 us
  transfers between devices with their start and end apart: 9, of which 9 were waited for; matrix products, arithmetic and copies ran while one was open for 5% of the time, Pallas kernels for 0%

commit v1 on v0

--- a/solution.py
+++ b/solution.py
@@ -1,6 +1,8 @@
 import jax
 import jax.numpy as jnp
 from jax import lax
+from jax.experimental import pallas as pl
+from jax.experimental.pallas import tpu as pltpu
 from jax.sharding import PartitionSpec as P
 
 D = 2048
@@ -80,6 +82,233 @@
     )
 
 
+def cast(values):
+    return values.astype(jnp.bfloat16)
+
+
+def swap(values, axis, mask):
+    size = lax.axis_size(axis)
+    return lax.ppermute(values, axis, [(i, i ^ mask) for i in range(size)])
+
+
+def assemble(pieces, orders):
+    count = sum(p.shape[0] for p in pieces[0])
+    _, half, width = pieces[0][0].shape
+    sizes = [[p.shape[0] for p in side] for side in pieces]
+
+    def kernel(*refs):
+        *sources, out = refs
+        sources = iter(sources)
+        for side, (order, lengths) in enumerate(zip(orders, sizes)):
+            at = 0
+            for length in lengths:
+                source = next(sources)
+                for i in range(length):
+                    j = order[at + i]
+                    out[side * half : (side + 1) * half, j * width : (j + 1) * width] = source[i]
+                at += length
+
+    flat = [p for side in pieces for p in side]
+    return pl.pallas_call(
+        kernel,
+        out_shape=jax.ShapeDtypeStruct((2 * half, count * width), flat[0].dtype),
+        in_specs=[pl.BlockSpec(memory_space=pltpu.VMEM)] * len(flat),
+        out_specs=pl.BlockSpec(memory_space=pltpu.VMEM),
+        compiler_params=pltpu.CompilerParams(vmem_limit_bytes=5 * half * count * width * 4),
+        cost_estimate=pl.CostEstimate(
+            flops=8 * half * count * width,
+            bytes_accessed=8 * half * count * width,
+            transcendentals=0,
+        ),
+    )(*flat)
+
+
+def gather_ra(block):
+    half = block.shape[0] // 2
+    top, low = [block[None, :half]], [block[None, half:]]
+    bits = [1 << b for b in range(lax.axis_size("ra").bit_length() - 1)]
+    top_order, low_order = [0], [0]
+    for up_bit, down_bit in zip(bits, reversed(bits)):
+        top_new = swap(top[0] if len(top) == 1 else jnp.concatenate(top), "ra", up_bit)
+        low_new = swap(low[0] if len(low) == 1 else jnp.concatenate(low), "ra", down_bit)
+        top_order += [j ^ up_bit for j in top_order]
+        low_order += [j ^ down_bit for j in low_order]
+        top.append(top_new)
+        low.append(low_new)
+    return assemble([top, low], [top_order, low_order])
+
+
+def reduce_ra(values, width):
+    half = values.shape[0] // 2
+    count = lax.axis_size("ra")
+    bits = [1 << b for b in range(count.bit_length() - 1)]
+    top = {j: values[:half, j * width : (j + 1) * width] for j in range(count)}
+    low = {j: values[half:, j * width : (j + 1) * width] for j in range(count)}
+
+    def halve(parts, bit):
+        keep = [j for j in parts if not j & bit]
+        sent = jnp.stack([cast(parts[j ^ bit]) for j in keep])
+        got = swap(sent, "ra", bit)
+        return {
+            j: parts[j].astype(jnp.float32) + got[at].astype(jnp.float32)
+            for at, j in enumerate(keep)
+        }
+
+    for up_bit, down_bit in zip(bits, reversed(bits)):
+        top = halve(top, down_bit)
+        low = halve(low, up_bit)
+    return jnp.concatenate([top[0], low[0]], axis=0)
+
+
+def sum_ra(values):
+    count = lax.axis_size("ra")
+    for b in range(count.bit_length() - 1):
+        values = values + swap(values, "ra", 1 << b)
+    return values
+
+
+def relative(blocks):
+    me = lax.axis_index("ra")
+    return [
+        lax.dynamic_index_in_dim(blocks, me ^ j, 0, keepdims=False)
+        for j in range(blocks.shape[0])
+    ]
+
+
+def lanes():
+    size = lax.axis_size("cb")
+    return [list(range(core, size, 2)) for core in range(2)]
+
+
+def exchange(chunks):
+    got = lax.all_to_all(chunks, "cb", 0, 0, axis_index_groups=lanes())
+    other = swap(got, "cb", 1)
+    south = lax.rem(lax.axis_index("cb"), 2) == 0
+    return jnp.stack([jnp.where(south, got, other), jnp.where(south, other, got)], axis=1)
+
+
+def reshard(weights):
+    rows, columns = weights[0].shape
+    chips = lax.axis_size("cb") // 2
+    chunks = jnp.stack(
+        [cast(w).reshape(rows, chips, columns // chips).transpose(1, 0, 2) for w in weights],
+        axis=1,
+    )
+    whole = exchange(chunks)
+    whole = whole.reshape(lax.axis_size("ra"), -1, *chunks.shape[1:])
+    parts = relative(whole)
+    return [
+        jnp.concatenate([piece[at] for part in parts for piece in part], axis=0)
+        for at in range(len(weights))
+    ]
+
+
+def hidden_slice(scale):
+    size = scale.shape[0] // (lax.axis_size("cb") // 2)
+    return lax.dynamic_slice_in_dim(scale, lax.axis_index("cb") // 2 * size, size, 0)
+
+
+def groups_of(chips):
+    return [[0], list(range(1, chips))]
+
+
+def row_norm(values, gain):
+    meansq = sum_ra(jnp.sum(values * values, axis=1)) / D
+    return values * lax.rsqrt(meansq + 1e-06)[:, None] * own_slice(gain, values.shape[1])
+
+
+def hidden_groups(own, w_gate, s_gate, w_up, s_up):
+    chips = lax.axis_size("cb") // 2
+    half = own.shape[0] // 2
+    s_gate, s_up = hidden_slice(s_gate), hidden_slice(s_up)
+    arrived = [own] + [swap(own, "cb", 2 * k) for k in range(1, chips)]
+    results = []
+    for members in groups_of(chips):
+        stacked = [arrived[k] for k in members]
+        block = jnp.concatenate(
+            [s[:half] for s in stacked] + [s[half:] for s in stacked], axis=0
+        )
+        normed = gather_ra(block)
+        gate = jnp.dot(normed, w_gate, preferred_element_type=jnp.float32)
+        upper = jnp.dot(normed, w_up, preferred_element_type=jnp.float32)
+        results.append(cast(jax.nn.silu(gate * s_gate) * (upper * s_up)))
+    return results
+
+
+def summed_down(hiddens, w_down, shape):
+    rows, width = shape
+    chips = lax.axis_size("cb") // 2
+    total = None
+    for members, hidden in reversed(list(zip(groups_of(chips), hiddens))):
+        product = lax.dot_general(
+            hidden, w_down, (((1,), (1,)), ((), ())), preferred_element_type=jnp.float32
+        )
+        summed = reduce_ra(cast(product), width)
+        summed = summed.reshape(2, len(members), rows // 2, width)
+        for at, k in enumerate(members):
+            part = summed[:, at].reshape(rows, width)
+            if k:
+                part = swap(cast(part), "cb", 2 * k).astype(jnp.float32)
+            total = part if total is None else total + part
+    return total
+
+
+def resharded(
+    tokens,
+    gain_first,
+    gate_first,
+    gate_first_scale,
+    up_first,
+    up_first_scale,
+    down_first,
+    down_first_scale,
+    gain_second,
+    gate_second,
+    gate_second_scale,
+    up_second,
+    up_second_scale,
+    down_second,
+    down_second_scale,
+    gain_last,
+):
+    shape = tokens.shape
+    width = shape[1]
+    start = tokens.astype(jnp.float32)
+    w_gate, w_up = reshard([gate_first, up_first])
+    w_gate, gate_second, up_second, down_second = lax.optimization_barrier(
+        (w_gate, gate_second, up_second, down_second)
+    )
+    (w_down,) = reshard([down_first.T])
+    hiddens = hidden_groups(
+        cast(row_norm(start, gain_first)), w_gate, gate_first_scale, w_up, up_first_scale
+    )
+    w_gate, w_up, w_down_second = reshard([gate_second, up_second, down_second.T])
+    b_first = summed_down(hiddens, w_down, shape)
+    first = 0.1 * start + 0.5 * b_first * own_slice(down_first_scale, width)
+    hiddens = hidden_groups(
+        cast(row_norm(first, gain_second)), w_gate, gate_second_scale, w_up, up_second_scale
+    )
+    second = 0.1 * first + 0.5 * summed_down(hiddens, w_down_second, shape) * own_slice(
+        down_second_scale, width
+    )
+    return cast(row_norm(second, gain_last))
+
+
+def plan_for(mesh):
+    ra, cb = mesh.shape["ra"], mesh.shape["cb"]
+
+    def run(tokens, *rest):
+        weight = rest[1]
+        activations = 4 * tokens.size * ra * cb // 2
+        weights = 6 * weight.size * cb
+        regular = cb % 2 == 0 and not (cb // 2) & (cb // 2 - 1) and not ra & (ra - 1)
+        if regular and activations < weights:
+            return resharded(tokens, *rest)
+        return shards(tokens, *rest)
+
+    return run
+
+
 def solution(mesh):
     placed = (
         P("cb", "ra"),
@@ -100,5 +329,5 @@
         P(),
     )
     return jax.shard_map(
-        shards, mesh=mesh, in_specs=placed, out_specs=P("cb", "ra"), check_vma=False
-    )
+        plan_for(mesh), mesh=mesh, in_specs=placed, out_specs=P("cb", "ra"), check_vma=False
+    )

time: 520 us -> 382 us (0.73)
  waiting for transfers between devices: 450 us -> 209 us
  starting transfers between devices: 0.33 us -> 87.8 us
  local copies, waits for them, and re-layouts: 1.31 us -> 23.3 us
  other arithmetic: 15.5 us -> 28.5 us
  between operations: 13.3 us -> 0.84 us
  blocking collectives: 8.93 us -> 0 us
    all_gather x7 -> x0, waiting for transfers between devices: 379 us -> none  [the longest x2 122 us: expand(): lax.all_gather(w_down.astype(jnp.bfloat16), 'cb', axis=1, tiled=True)]
    ppermute x0 -> x53, waiting for transfers between devices: none -> 200 us  [swap(): return lax.ppermute(values, axis, [(i, i ^ mask) for i in range(size)])]
    ppermute x0 -> x53, starting transfers between devices: none -> 74.5 us  [swap(): return lax.ppermute(values, axis, [(i, i ^ mask) for i in range(size)])]
    psum x1 -> x0, waiting for transfers between devices: 46.2 us -> none  [shards(): lax.psum(partial_value.astype(jnp.bfloat16), 'ra').astype(jnp.float32)]
    reduce_scatter x1 -> x0, waiting for transfers between devices: 24.8 us -> none  [reduce_share(): lax.psum_scatter(partial_value.astype(jnp.bfloat16), 'ra', scatter_dimens...]
    another operation x0 -> x25, other arithmetic: none -> 14 us  [the longest x7 7.66 us: exchange(): jnp.stack([jnp.where(south, got, other), jnp.where(south, other, got)], a...]
    all_to_all x0 -> x3, starting transfers between devices: none -> 13.3 us  [exchange(): got = lax.all_to_all(chunks, 'cb', 0, 0, axis_index_groups=lanes())]
    all_to_all x0 -> x3, waiting for transfers between devices: none -> 9.48 us  [exchange(): got = lax.all_to_all(chunks, 'cb', 0, 0, axis_index_groups=lanes())]
  transfers between devices with their start and end apart: 9 -> 56, of which waited for: 9 -> 35; matrix products, arithmetic and copies ran while one was open for 5% -> 12% of each run, Pallas kernels for 0% -> 0%
where the time goes in v1:
time: 382 us; the launch traced here: 381 us
  waiting for transfers between devices  209 us (55%)
  starting transfers between devices  87.8 us (23%)
  matrix products  30.5 us (8%)
  other arithmetic  28.5 us (7%)
  local copies, waits for them, and re-layouts  23.3 us (6%)
    ppermute x53, waiting for transfers between devices, swap(): return lax.ppermute(values, axis, [(i, i ^ mask) for i in range(size)])  200 us
    ppermute x53, starting transfers between devices, swap(): return lax.ppermute(values, axis, [(i, i ^ mask) for i in range(size)])  74.5 us
    dot_general x4, matrix products, summed_down(): lax.dot_general(hidden, w_down, (((1,), (1,)), ((), ())), preferred_eleme...  23.1 us
    all_to_all x3, starting transfers between devices, exchange(): got = lax.all_to_all(chunks, 'cb', 0, 0, axis_index_groups=lanes())  13.3 us
    all_to_all x3, waiting for transfers between devices, exchange(): got = lax.all_to_all(chunks, 'cb', 0, 0, axis_index_groups=lanes())  9.48 us
    another operation x7, other arithmetic, exchange(): jnp.stack([jnp.where(south, got, other), jnp.where(south, other, got)], a...  7.66 us
  transfers between devices with their start and end apart: 56, of which 35 were waited for; matrix products, arithmetic and copies ran while one was open for 12% of the time, Pallas kernels for 0%

profile of v1, /device:TPU:0, one launch (start us, length us, event | category | flops | bytes accessed | tf_op | source)
XLA Modules:
  0.0 380.5 jit_solution(14160519159907719463)
XLA Ops:
  1.1 3.0 collective-permute-start
  10.4 4.2 %collective-permute-start.4 = (bf16[256,512]{1,0:T(8,128)(2,1)S(1)}, bf16[256,512]{1,0:T(8,128)(2,1)}, u32[]{:S(2)}, u32[]{:S(2)}) collective-permute-start(bf16[256,512]{1,0:T(8,128)(2,1)S(1)} %fusion.20), channel_id=1, source_target_pairs={{0,6},{1,7},{2,4},{3,5},{4,2},{5,3},{6,0},{7,1},{8,14},{9,15},{10,... | collective-permute-start | bytes 786440 | tf_op jit(solution)/shard_map/ppermute | solution.py:91
  16.8 4.2 %all-to-all-start.1 = ((bf16[4,1,256,352]{2,3,1,0:T(8,128)(2,1)}), bf16[4,1,256,352]{2,3,1,0:T(8,128)(2,1)}, u32[]{:S(2)}, u32[]{:S(2)}) async-start(bf16[4,1,256,352]{2,3,1,0:T(8,128)(2,1)} %bitcast.30), calls=%async_computation.1 | async-start | bytes 1441792 | tf_op jit(solution)/shard_map/all_to_all | solution.py:184
  26.0 17.3 %collective-permute-done.3 = bf16[256,512]{1,0:T(8,128)(2,1)} collective-permute-done((bf16[256,512]{1,0:T(8,128)(2,1)S(1)}, bf16[256,512]{1,0:T(8,128)(2,1)}, u32[]{:S(2)}, u32[]{:S(2)}) %collective-permute-start.3) | collective-permute-done | bytes 262176 | tf_op jit(solution)/shard_map/ppermute | solution.py:91
  50.1 4.3 %all-to-all-start = ((bf16[4,2,256,352]{2,3,1,0:T(8,128)(2,1)}), bf16[4,2,256,352]{2,3,1,0:T(8,128)(2,1)}, u32[]{:S(2)}, u32[]{:S(2)}) async-start(bf16[4,2,256,352]{2,3,1,0:T(8,128)(2,1)} %copy.72), calls=%async_computation | async-start | bytes 2883584 | tf_op jit(solution)/shard_map/all_to_all | solution.py:184
  60.9 13.3 %collective-permute-done.6.refs_2_ = bf16[2,384,512]{2,1,0:T(8,128)(2,1)S(1)} collective-permute-done((bf16[2,384,512]{2,1,0:T(8,128)(2,1)}, bf16[2,384,512]{2,1,0:T(8,128)(2,1)S(1)}, u32[]{:S(2)}, u32[]{:S(2)}) %collective-permute-start.6) | collective-permute-done | bytes 786464 | tf_op jit(solution)/shard_map/ppermute | solution.py:91
  80.0 8.3 %all-to-all-done = bf16[4,2,256,352]{2,3,1,0:T(8,128)(2,1)} async-done(((bf16[4,2,256,352]{2,3,1,0:T(8,128)(2,1)}), bf16[4,2,256,352]{2,3,1,0:T(8,128)(2,1)}, u32[]{:S(2)}, u32[]{:S(2)}) %all-to-all-start) | async-done | bytes 1441824 | tf_op jit(solution)/shard_map/all_to_all | solution.py:184
  88.4 3.3 collective-permute-done.9
  98.7 7.6 %convolution_convert_fusion.1 = bf16[768,2048]{1,0:T(8,128)(2,1)} fusion(bf16[2048,352]{0,1:T(8,128)(2,1)} %copy-done.12, f32[768,352]{0,1:T(8,128)} %convolution_multiply_fusion.2, bf16[768,2048]{1,0:T(8,128)(2,1)S(1)} %copy-done.1, bf16[2048,352]{0,1:T(8,128)(2,1)} %copy-done.14, f32[352]{0:T(512)S(1)} %dynamic_slice.71), kind=kOutput, calls=%fused_computation.17 | convolution fusion | flops 2218057728 | bytes 10257792 | tf_op jit(solution)/shard_map/dot_general | solution.py:243
  112.1 3.3 collective-permute-done.18.refs_1_
  116.0 16.0 %collective-permute-done.20.refs_4_ = bf16[1,128,512]{2,1,0:T(8,128)(2,1)S(1)} collective-permute-done((bf16[1,128,512]{2,1,0:T(8,128)(2,1)S(1)}, bf16[1,128,512]{2,1,0:T(8,128)(2,1)S(1)}, u32[]{:S(2)}, u32[]{:S(2)}) %collective-permute-start.20) | collective-permute-done | bytes 131104 | tf_op jit(solution)/shard_map/ppermute | solution.py:91
  133.5 3.2 collective-permute-done.19.refs_2_
  147.4 4.8 %all-to-all-start.2 = ((bf16[4,3,256,352]{2,3,1,0:T(8,128)(2,1)}), bf16[4,3,256,352]{2,3,1,0:T(8,128)(2,1)}, u32[]{:S(2)}, u32[]{:S(2)}) async-start(bf16[4,3,256,352]{2,3,1,0:T(8,128)(2,1)} %copy.87), calls=%async_computation.2 | async-start | bytes 4325376 | tf_op jit(solution)/shard_map/all_to_all | solution.py:184
  156.3 4.0 %convolution_convert_fusion.3 = bf16[256,2048]{1,0:T(8,128)(2,1)S(1)} fusion(bf16[2048,352]{0,1:T(8,128)(2,1)} %copy-done.12, f32[256,352]{0,1:T(8,128)} %convolution_multiply_fusion.6, bf16[256,2048]{1,0:T(8,128)(2,1)S(1)} %shard_map.155, bf16[2048,352]{0,1:T(8,128)(2,1)} %copy-done.14, f32[352]{0:T(512)S(1)} %dynamic_slice.71), kind=kOutput, calls=%fused_computation.19 | convolution fusion | flops 739352576 | bytes 5342592 | tf_op jit(solution)/shard_map/dot_general | solution.py:243
  163.1 12.7 %collective-permute-done.13 = bf16[2,384,512]{2,1,0:T(8,128)(2,1)} collective-permute-done((bf16[2,384,512]{2,1,0:T(8,128)(2,1)S(1)}, bf16[2,384,512]{2,1,0:T(8,128)(2,1)}, u32[]{:S(2)}, u32[]{:S(2)}) %collective-permute-start.13) | collective-permute-done | bytes 786464 | tf_op jit(solution)/shard_map/ppermute | solution.py:91
  179.8 4.0 %collective-permute-done.23 = bf16[1,128,512]{2,1,0:T(8,128)(2,1)S(1)} collective-permute-done((bf16[1,128,512]{2,1,0:T(8,128)(2,1)S(1)}, bf16[1,128,512]{2,1,0:T(8,128)(2,1)S(1)}, u32[]{:S(2)}, u32[]{:S(2)}) %collective-permute-start.23) | collective-permute-done | bytes 131104 | tf_op jit(solution)/shard_map/ppermute | solution.py:91
  186.7 3.2 collective-permute-start.17
  192.0 6.0 %collective-permute-done.17 = bf16[256,512]{1,0:T(8,128)(2,1)S(1)} collective-permute-done((bf16[256,512]{1,0:T(8,128)(2,1)S(1)}, bf16[256,512]{1,0:T(8,128)(2,1)S(1)}, u32[]{:S(2)}, u32[]{:S(2)}) %collective-permute-start.17) | collective-permute-done | bytes 262176 | tf_op jit(solution)/shard_map/ppermute | solution.py:91
  198.0 23.8 %collective-permute-done.16 = bf16[256,512]{1,0:T(8,128)(2,1)S(1)} collective-permute-done((bf16[256,512]{1,0:T(8,128)(2,1)S(1)}, bf16[256,512]{1,0:T(8,128)(2,1)S(1)}, u32[]{:S(2)}, u32[]{:S(2)}) %collective-permute-start.16) | collective-permute-done | bytes 262176 | tf_op jit(solution)/shard_map/ppermute | solution.py:91
  233.9 6.6 %collective-permute-done.30 = bf16[256,512]{1,0:T(8,128)(2,1)S(1)} collective-permute-done((bf16[256,512]{1,0:T(8,128)(2,1)S(1)}, bf16[256,512]{1,0:T(8,128)(2,1)S(1)}, u32[]{:S(2)}, u32[]{:S(2)}) %collective-permute-start.30) | collective-permute-done | bytes 262176 | tf_op jit(solution)/shard_map/ppermute | solution.py:91
  240.5 9.1 %collective-permute-done.29 = bf16[256,512]{1,0:T(8,128)(2,1)S(1)} collective-permute-done((bf16[256,512]{1,0:T(8,128)(2,1)S(1)}, bf16[256,512]{1,0:T(8,128)(2,1)S(1)}, u32[]{:S(2)}, u32[]{:S(2)}) %collective-permute-start.29) | collective-permute-done | bytes 262176 | tf_op jit(solution)/shard_map/ppermute | solution.py:91
  251.9 6.5 %collective-permute-done.31.refs_1_ = bf16[1,384,512]{2,1,0:T(8,128)(2,1)S(1)} collective-permute-done((bf16[1,384,512]{2,1,0:T(8,128)(2,1)S(1)}, bf16[1,384,512]{2,1,0:T(8,128)(2,1)S(1)}, u32[]{:S(2)}, u32[]{:S(2)}) %collective-permute-start.31) | collective-permute-done | bytes 393248 | tf_op jit(solution)/shard_map/ppermute | solution.py:91
  265.2 9.8 %collective-permute-done.32.refs_2_ = bf16[2,384,512]{2,1,0:T(8,128)(2,1)S(1)} collective-permute-done((bf16[2,384,512]{2,1,0:T(8,128)(2,1)S(1)}, bf16[2,384,512]{2,1,0:T(8,128)(2,1)S(1)}, u32[]{:S(2)}, u32[]{:S(2)}) %collective-permute-start.32) | collective-permute-done | bytes 786464 | tf_op jit(solution)/shard_map/ppermute | solution.py:91
  282.7 7.6 %convolution_convert_fusion = bf16[768,2048]{1,0:T(8,128)(2,1)} fusion(bf16[2048,352]{0,1:T(8,128)(2,1)} %copy-done.13, f32[768,352]{0,1:T(8,128)} %convolution_multiply_fusion, bf16[768,2048]{1,0:T(8,128)(2,1)S(1)} %shard_map.156, bf16[2048,352]{0,1:T(8,128)(2,1)} %copy-done.15, f32[352]{0:T(512)S(1)} %dynamic_slice.83), kind=kOutput, calls=%fused_computation.16 | convolution fusion | flops 2218057728 | bytes 10257792 | tf_op jit(solution)/shard_map/dot_general | solution.py:243
  298.8 13.5 %collective-permute-done.45.refs_4_ = bf16[1,128,512]{2,1,0:T(8,128)(2,1)S(1)} collective-permute-done((bf16[1,128,512]{2,1,0:T(8,128)(2,1)S(1)}, bf16[1,128,512]{2,1,0:T(8,128)(2,1)S(1)}, u32[]{:S(2)}, u32[]{:S(2)}) %collective-permute-start.45) | collective-permute-done | bytes 131104 | tf_op jit(solution)/shard_map/ppermute | solution.py:91
  315.2 4.5 %collective-permute-done.46.refs_5_ = bf16[2,128,512]{2,1,0:T(8,128)(2,1)S(1)} collective-permute-done((bf16[2,128,512]{2,1,0:T(8,128)(2,1)S(1)}, bf16[2,128,512]{2,1,0:T(8,128)(2,1)S(1)}, u32[]{:S(2)}, u32[]{:S(2)}) %collective-permute-start.46) | collective-permute-done | bytes 262176 | tf_op jit(solution)/shard_map/ppermute | solution.py:91
  321.1 7.0 %collective-permute-done.37 = bf16[1,384,512]{2,1,0:T(8,128)(2,1)S(1)} collective-permute-done((bf16[1,384,512]{2,1,0:T(8,128)(2,1)S(1)}, bf16[1,384,512]{2,1,0:T(8,128)(2,1)S(1)}, u32[]{:S(2)}, u32[]{:S(2)}) %collective-permute-start.37) | collective-permute-done | bytes 393248 | tf_op jit(solution)/shard_map/ppermute | solution.py:91
  330.8 4.0 %convolution_convert_fusion.2 = bf16[256,2048]{1,0:T(8,128)(2,1)S(1)} fusion(bf16[2048,352]{0,1:T(8,128)(2,1)} %copy-done.13, f32[256,352]{0,1:T(8,128)} %convolution_multiply_fusion.4, bf16[256,2048]{1,0:T(8,128)(2,1)S(1)} %shard_map.157, bf16[2048,352]{0,1:T(8,128)(2,1)} %copy-done.15, f32[352]{0:T(512)S(1)} %dynamic_slice.83), kind=kOutput, calls=%fused_computation.18 | convolution fusion | flops 739352576 | bytes 5342592 | tf_op jit(solution)/shard_map/dot_general | solution.py:243
  336.6 7.7 %collective-permute-done.38 = bf16[2,384,512]{2,1,0:T(8,128)(2,1)} collective-permute-done((bf16[2,384,512]{2,1,0:T(8,128)(2,1)S(1)}, bf16[2,384,512]{2,1,0:T(8,128)(2,1)}, u32[]{:S(2)}, u32[]{:S(2)}) %collective-permute-start.38) | collective-permute-done | bytes 786464 | tf_op jit(solution)/shard_map/ppermute | solution.py:91
  354.7 5.6 %collective-permute-start.42 = (bf16[256,512]{1,0:T(8,128)(2,1)S(1)}, bf16[256,512]{1,0:T(8,128)(2,1)S(1)}, u32[]{:S(2)}, u32[]{:S(2)}) collective-permute-start(bf16[256,512]{1,0:T(8,128)(2,1)S(1)} %bitcast.532), channel_id=1, source_target_pairs={{0,6},{1,7},{2,4},{3,5},{4,2},{5,3},{6,0},{7,1},{8,14},{9,15},{10,... | collective-permute-start | bytes 786440 | tf_op jit(solution)/shard_map/ppermute | solution.py:91
  361.8 3.1 collective-permute-done.42
  364.9 7.3 %collective-permute-done.41 = bf16[256,512]{1,0:T(8,128)(2,1)S(1)} collective-permute-done((bf16[256,512]{1,0:T(8,128)(2,1)S(1)}, bf16[256,512]{1,0:T(8,128)(2,1)S(1)}, u32[]{:S(2)}, u32[]{:S(2)}) %collective-permute-start.41) | collective-permute-done | bytes 262176 | tf_op jit(solution)/shard_map/ppermute | solution.py:91
  (239 shorter events, 141.0 us)
Async XLA Ops:
  10.4 14.7 %collective-permute-start.4 = (bf16[256,512]{1,0:T(8,128)(2,1)S(1)}, bf16[256,512]{1,0:T(8,128)(2,1)}, u32[]{:S(2)}, u32[]{:S(2)}) collective-permute-start(bf16[256,512]{1,0:T(8,128)(2,1)S(1)} %fusion.20), channel_id=1, source_target_pairs={{0,6},{1,7},{2,4},{3,5},{4,2},{5,3},{6,0},{7,1},{8,14},{9,15},{10,... | collective-permute-start | bytes 786440 | tf_op jit(solution)/shard_map/ppermute | solution.py:91
  14.5 28.8 %collective-permute-start.3 = (bf16[256,512]{1,0:T(8,128)(2,1)S(1)}, bf16[256,512]{1,0:T(8,128)(2,1)}, u32[]{:S(2)}, u32[]{:S(2)}) collective-permute-start(bf16[256,512]{1,0:T(8,128)(2,1)S(1)} %fusion.20), channel_id=1, source_target_pairs={{0,4},{1,5},{2,6},{3,7},{4,0},{5,1},{6,2},{7,3},{8,12},{9,13},{10,... | collective-permute-start | bytes 786440 | tf_op jit(solution)/shard_map/ppermute | solution.py:91
  16.8 33.3 %all-to-all-start.1 = ((bf16[4,1,256,352]{2,3,1,0:T(8,128)(2,1)}), bf16[4,1,256,352]{2,3,1,0:T(8,128)(2,1)}, u32[]{:S(2)}, u32[]{:S(2)}) async-start(bf16[4,1,256,352]{2,3,1,0:T(8,128)(2,1)} %bitcast.30), calls=%async_computation.1 | async-start | bytes 1441792 | tf_op jit(solution)/shard_map/all_to_all | solution.py:184
  23.0 21.4 %collective-permute-start.2 = (bf16[256,512]{1,0:T(8,128)(2,1)S(1)}, bf16[256,512]{1,0:T(8,128)(2,1)S(1)}, u32[]{:S(2)}, u32[]{:S(2)}) collective-permute-start(bf16[256,512]{1,0:T(8,128)(2,1)S(1)} %fusion.20), channel_id=1, source_target_pairs={{0,2},{1,3},{2,0},{3,1},{4,6},{5,7},{6,4},{7,5},{8,10},{9,11},{10,... | collective-permute-start | bytes 786440 | tf_op jit(solution)/shard_map/ppermute | solution.py:91
  50.1 38.2 %all-to-all-start = ((bf16[4,2,256,352]{2,3,1,0:T(8,128)(2,1)}), bf16[4,2,256,352]{2,3,1,0:T(8,128)(2,1)}, u32[]{:S(2)}, u32[]{:S(2)}) async-start(bf16[4,2,256,352]{2,3,1,0:T(8,128)(2,1)} %copy.72), calls=%async_computation | async-start | bytes 2883584 | tf_op jit(solution)/shard_map/all_to_all | solution.py:184
  55.4 18.8 %collective-permute-start.6 = (bf16[2,384,512]{2,1,0:T(8,128)(2,1)}, bf16[2,384,512]{2,1,0:T(8,128)(2,1)S(1)}, u32[]{:S(2)}, u32[]{:S(2)}) collective-permute-start(bf16[2,384,512]{2,1,0:T(8,128)(2,1)} %pad_maximum_fusion.2), channel_id=1, source_target_pairs={{0,16},{8,24},{16,0},{24,8},{1,17},{9,25},{17,1},{25,9},{2,18},{10... | collective-permute-start | bytes 2359304 | tf_op jit(solution)/shard_map/ppermute | solution.py:91
  57.9 18.5 %collective-permute-start.8 = (bf16[2,384,512]{2,1,0:T(8,128)(2,1)}, bf16[2,384,512]{2,1,0:T(8,128)(2,1)S(1)}, u32[]{:S(2)}, u32[]{:S(2)}) collective-permute-start(bf16[2,384,512]{2,1,0:T(8,128)(2,1)} %pad_maximum_fusion.3), channel_id=1, source_target_pairs={{0,8},{8,0},{16,24},{24,16},{1,9},{9,1},{17,25},{25,17},{2,10},{10... | collective-permute-start | bytes 2359304 | tf_op jit(solution)/shard_map/ppermute | solution.py:91
  59.4 17.3 %collective-permute-start.10 = (bf16[4,1,256,352]{2,3,0,1:T(8,128)(2,1)}, bf16[4,1,256,352]{2,3,0,1:T(8,128)(2,1)}, u32[]{:S(2)}, u32[]{:S(2)}) collective-permute-start(bf16[4,1,256,352]{2,3,0,1:T(8,128)(2,1)} %bitcast.31), channel_id=1, source_target_pairs={{0,1},{1,0},{2,3},{3,2},{4,5},{5,4},{6,7},{7,6},{8,9},{9,8},{10,11... | collective-permute-start | bytes 2162696 | tf_op jit(solution)/shard_map/ppermute | solution.py:91
  108.5 33.6 %collective-permute-start.11 = (bf16[2,384,512]{2,1,0:T(8,128)(2,1)}, bf16[2,384,512]{2,1,0:T(8,128)(2,1)}, u32[]{:S(2)}, u32[]{:S(2)}) collective-permute-start(bf16[2,384,512]{2,1,0:T(8,128)(2,1)} %pad_maximum_fusion.4), channel_id=1, source_target_pairs={{0,16},{8,24},{16,0},{24,8},{1,17},{9,25},{17,1},{25,9},{2,18},{10... | collective-permute-start | bytes 2359304 | tf_op jit(solution)/shard_map/ppermute | solution.py:91
  111.6 20.3 %collective-permute-start.20 = (bf16[1,128,512]{2,1,0:T(8,128)(2,1)S(1)}, bf16[1,128,512]{2,1,0:T(8,128)(2,1)S(1)}, u32[]{:S(2)}, u32[]{:S(2)}) collective-permute-start(bf16[1,128,512]{2,1,0:T(8,128)(2,1)S(1)} %get-tuple-element.111.refs_3_), channel_id=1, source_target_pairs={{0,16},{8,24},{16,0},{24,8},{1,17},{9,25},{17,1},{25,9},{2,18},{10... | collective-permute-start | bytes 393224 | tf_op jit(solution)/shard_map/ppermute | solution.py:91
  115.4 21.3 %collective-permute-start.19 = (bf16[2,128,512]{2,1,0:T(8,128)(2,1)S(1)}, bf16[2,128,512]{2,1,0:T(8,128)(2,1)S(1)}, u32[]{:S(2)}, u32[]{:S(2)}) collective-permute-start(bf16[2,128,512]{2,1,0:T(8,128)(2,1)S(1)} %pad_maximum_fusion.10), channel_id=1, source_target_pairs={{0,16},{8,24},{16,0},{24,8},{1,17},{9,25},{17,1},{25,9},{2,18},{10... | collective-permute-start | bytes 786440 | tf_op jit(solution)/shard_map/ppermute | solution.py:91
  147.4 86.5 %all-to-all-start.2 = ((bf16[4,3,256,352]{2,3,1,0:T(8,128)(2,1)}), bf16[4,3,256,352]{2,3,1,0:T(8,128)(2,1)}, u32[]{:S(2)}, u32[]{:S(2)}) async-start(bf16[4,3,256,352]{2,3,1,0:T(8,128)(2,1)} %copy.87), calls=%async_computation.2 | async-start | bytes 4325376 | tf_op jit(solution)/shard_map/all_to_all | solution.py:184
  155.2 20.6 %collective-permute-start.13 = (bf16[2,384,512]{2,1,0:T(8,128)(2,1)S(1)}, bf16[2,384,512]{2,1,0:T(8,128)(2,1)}, u32[]{:S(2)}, u32[]{:S(2)}) collective-permute-start(bf16[2,384,512]{2,1,0:T(8,128)(2,1)S(1)} %pad_maximum_fusion.5), channel_id=1, source_target_pairs={{0,8},{8,0},{16,24},{24,16},{1,9},{9,1},{17,25},{25,17},{2,10},{10... | collective-permute-start | bytes 2359304 | tf_op jit(solution)/shard_map/ppermute | solution.py:91
  160.4 18.3 %collective-permute-start.22 = (bf16[2,128,512]{2,1,0:T(8,128)(2,1)S(1)}, bf16[2,128,512]{2,1,0:T(8,128)(2,1)S(1)}, u32[]{:S(2)}, u32[]{:S(2)}) collective-permute-start(bf16[2,128,512]{2,1,0:T(8,128)(2,1)S(1)} %pad_maximum_fusion.12), channel_id=1, source_target_pairs={{0,16},{8,24},{16,0},{24,8},{1,17},{9,25},{17,1},{25,9},{2,18},{10... | collective-permute-start | bytes 786440 | tf_op jit(solution)/shard_map/ppermute | solution.py:91
  162.0 17.8 %collective-permute-start.24 = (bf16[2,128,512]{2,1,0:T(8,128)(2,1)S(1)}, bf16[2,128,512]{2,1,0:T(8,128)(2,1)S(1)}, u32[]{:S(2)}, u32[]{:S(2)}) collective-permute-start(bf16[2,128,512]{2,1,0:T(8,128)(2,1)S(1)} %pad_maximum_fusion.13), channel_id=1, source_target_pairs={{0,8},{8,0},{16,24},{24,16},{1,9},{9,1},{17,25},{25,17},{2,10},{10... | collective-permute-start | bytes 786440 | tf_op jit(solution)/shard_map/ppermute | solution.py:91
  186.7 11.3 %collective-permute-start.17 = (bf16[256,512]{1,0:T(8,128)(2,1)S(1)}, bf16[256,512]{1,0:T(8,128)(2,1)S(1)}, u32[]{:S(2)}, u32[]{:S(2)}) collective-permute-start(bf16[256,512]{1,0:T(8,128)(2,1)S(1)} %bitcast.531), channel_id=1, source_target_pairs={{0,6},{1,7},{2,4},{3,5},{4,2},{5,3},{6,0},{7,1},{8,14},{9,15},{10,... | collective-permute-start | bytes 786440 | tf_op jit(solution)/shard_map/ppermute | solution.py:91
  189.9 31.9 %collective-permute-start.16 = (bf16[256,512]{1,0:T(8,128)(2,1)S(1)}, bf16[256,512]{1,0:T(8,128)(2,1)S(1)}, u32[]{:S(2)}, u32[]{:S(2)}) collective-permute-start(bf16[256,512]{1,0:T(8,128)(2,1)S(1)} %bitcast.529), channel_id=1, source_target_pairs={{0,4},{1,5},{2,6},{3,7},{4,0},{5,1},{6,2},{7,3},{8,12},{9,13},{10,... | collective-permute-start | bytes 786440 | tf_op jit(solution)/shard_map/ppermute | solution.py:91
  189.9 31.9 %collective-permute-start.15 = (bf16[256,512]{1,0:T(8,128)(2,1)S(1)}, bf16[256,512]{1,0:T(8,128)(2,1)S(1)}, u32[]{:S(2)}, u32[]{:S(2)}) collective-permute-start(bf16[256,512]{1,0:T(8,128)(2,1)S(1)} %bitcast.527), channel_id=1, source_target_pairs={{0,2},{1,3},{2,0},{3,1},{4,6},{5,7},{6,4},{7,5},{8,10},{9,11},{10,... | collective-permute-start | bytes 786440 | tf_op jit(solution)/shard_map/ppermute | solution.py:91
  231.0 18.6 %collective-permute-start.29 = (bf16[256,512]{1,0:T(8,128)(2,1)S(1)}, bf16[256,512]{1,0:T(8,128)(2,1)S(1)}, u32[]{:S(2)}, u32[]{:S(2)}) collective-permute-start(bf16[256,512]{1,0:T(8,128)(2,1)S(1)} %multiply_convert_fusion.5), channel_id=1, source_target_pairs={{0,4},{1,5},{2,6},{3,7},{4,0},{5,1},{6,2},{7,3},{8,12},{9,13},{10,... | collective-permute-start | bytes 786440 | tf_op jit(solution)/shard_map/ppermute | solution.py:91
  231.0 18.6 %collective-permute-start.28 = (bf16[256,512]{1,0:T(8,128)(2,1)S(1)}, bf16[256,512]{1,0:T(8,128)(2,1)S(1)}, u32[]{:S(2)}, u32[]{:S(2)}) collective-permute-start(bf16[256,512]{1,0:T(8,128)(2,1)S(1)} %multiply_convert_fusion.5), channel_id=1, source_target_pairs={{0,2},{1,3},{2,0},{3,1},{4,6},{5,7},{6,4},{7,5},{8,10},{9,11},{10,... | collective-permute-start | bytes 786440 | tf_op jit(solution)/shard_map/ppermute | solution.py:91
  233.9 41.4 %collective-permute-start.35 = (bf16[4,3,256,352]{2,3,1,0:T(8,128)(2,1)}, bf16[4,3,256,352]{2,3,1,0:T(8,128)(2,1)S(1)}, u32[]{:S(2)}, u32[]{:S(2)}) collective-permute-start(bf16[4,3,256,352]{2,3,1,0:T(8,128)(2,1)} %all-to-all-done.2), channel_id=1, source_target_pairs={{0,1},{1,0},{2,3},{3,2},{4,5},{5,4},{6,7},{7,6},{8,9},{9,8},{10,11... | collective-permute-start | bytes 6488072 | tf_op jit(solution)/shard_map/ppermute | solution.py:91
  258.5 16.5 %collective-permute-start.32 = (bf16[2,384,512]{2,1,0:T(8,128)(2,1)S(1)}, bf16[2,384,512]{2,1,0:T(8,128)(2,1)S(1)}, u32[]{:S(2)}, u32[]{:S(2)}) collective-permute-start(bf16[2,384,512]{2,1,0:T(8,128)(2,1)S(1)} %pad_maximum_fusion.6), channel_id=1, source_target_pairs={{0,16},{8,24},{16,0},{24,8},{1,17},{9,25},{17,1},{25,9},{2,18},{10... | collective-permute-start | bytes 2359304 | tf_op jit(solution)/shard_map/ppermute | solution.py:91
  261.2 13.8 %collective-permute-start.34 = (bf16[2,384,512]{2,1,0:T(8,128)(2,1)S(1)}, bf16[2,384,512]{2,1,0:T(8,128)(2,1)S(1)}, u32[]{:S(2)}, u32[]{:S(2)}) collective-permute-start(bf16[2,384,512]{2,1,0:T(8,128)(2,1)S(1)} %pad_maximum_fusion.7), channel_id=1, source_target_pairs={{0,8},{8,0},{16,24},{24,16},{1,9},{9,1},{17,25},{25,17},{2,10},{10... | collective-permute-start | bytes 2359304 | tf_op jit(solution)/shard_map/ppermute | solution.py:91
  291.6 22.9 %collective-permute-start.36 = (bf16[2,384,512]{2,1,0:T(8,128)(2,1)S(1)}, bf16[2,384,512]{2,1,0:T(8,128)(2,1)S(1)}, u32[]{:S(2)}, u32[]{:S(2)}) collective-permute-start(bf16[2,384,512]{2,1,0:T(8,128)(2,1)S(1)} %pad_maximum_fusion.8), channel_id=1, source_target_pairs={{0,16},{8,24},{16,0},{24,8},{1,17},{9,25},{17,1},{25,9},{2,18},{10... | collective-permute-start | bytes 2359304 | tf_op jit(solution)/shard_map/ppermute | solution.py:91
  294.8 17.6 %collective-permute-start.45 = (bf16[1,128,512]{2,1,0:T(8,128)(2,1)S(1)}, bf16[1,128,512]{2,1,0:T(8,128)(2,1)S(1)}, u32[]{:S(2)}, u32[]{:S(2)}) collective-permute-start(bf16[1,128,512]{2,1,0:T(8,128)(2,1)S(1)} %get-tuple-element.103.refs_3_), channel_id=1, source_target_pairs={{0,16},{8,24},{16,0},{24,8},{1,17},{9,25},{17,1},{25,9},{2,18},{10... | collective-permute-start | bytes 393224 | tf_op jit(solution)/shard_map/ppermute | solution.py:91
  298.3 16.9 %collective-permute-start.44 = (bf16[2,128,512]{2,1,0:T(8,128)(2,1)S(1)}, bf16[2,128,512]{2,1,0:T(8,128)(2,1)S(1)}, u32[]{:S(2)}, u32[]{:S(2)}) collective-permute-start(bf16[2,128,512]{2,1,0:T(8,128)(2,1)S(1)} %pad_maximum_fusion.14), channel_id=1, source_target_pairs={{0,16},{8,24},{16,0},{24,8},{1,17},{9,25},{17,1},{25,9},{2,18},{10... | collective-permute-start | bytes 786440 | tf_op jit(solution)/shard_map/ppermute | solution.py:91
  314.7 13.5 %collective-permute-start.37 = (bf16[1,384,512]{2,1,0:T(8,128)(2,1)S(1)}, bf16[1,384,512]{2,1,0:T(8,128)(2,1)S(1)}, u32[]{:S(2)}, u32[]{:S(2)}) collective-permute-start(bf16[1,384,512]{2,1,0:T(8,128)(2,1)S(1)} %fusion.26), channel_id=1, source_target_pairs={{0,8},{8,0},{16,24},{24,16},{1,9},{9,1},{17,25},{25,17},{2,10},{10... | collective-permute-start | bytes 1179656 | tf_op jit(solution)/shard_map/ppermute | solution.py:91
  328.5 15.8 %collective-permute-start.38 = (bf16[2,384,512]{2,1,0:T(8,128)(2,1)S(1)}, bf16[2,384,512]{2,1,0:T(8,128)(2,1)}, u32[]{:S(2)}, u32[]{:S(2)}) collective-permute-start(bf16[2,384,512]{2,1,0:T(8,128)(2,1)S(1)} %pad_maximum_fusion.9), channel_id=1, source_target_pairs={{0,8},{8,0},{16,24},{24,16},{1,9},{9,1},{17,25},{25,17},{2,10},{10... | collective-permute-start | bytes 2359304 | tf_op jit(solution)/shard_map/ppermute | solution.py:91
  334.9 12.2 %collective-permute-start.47 = (bf16[2,128,512]{2,1,0:T(8,128)(2,1)S(1)}, bf16[2,128,512]{2,1,0:T(8,128)(2,1)S(1)}, u32[]{:S(2)}, u32[]{:S(2)}) collective-permute-start(bf16[2,128,512]{2,1,0:T(8,128)(2,1)S(1)} %pad_maximum_fusion.16), channel_id=1, source_target_pairs={{0,16},{8,24},{16,0},{24,8},{1,17},{9,25},{17,1},{25,9},{2,18},{10... | collective-permute-start | bytes 786440 | tf_op jit(solution)/shard_map/ppermute | solution.py:91
  336.5 12.7 %collective-permute-start.49 = (bf16[2,128,512]{2,1,0:T(8,128)(2,1)S(1)}, bf16[2,128,512]{2,1,0:T(8,128)(2,1)S(1)}, u32[]{:S(2)}, u32[]{:S(2)}) collective-permute-start(bf16[2,128,512]{2,1,0:T(8,128)(2,1)S(1)} %pad_maximum_fusion.17), channel_id=1, source_target_pairs={{0,8},{8,0},{16,24},{24,16},{1,9},{9,1},{17,25},{25,17},{2,10},{10... | collective-permute-start | bytes 786440 | tf_op jit(solution)/shard_map/ppermute | solution.py:91
  360.4 11.8 %collective-permute-start.41 = (bf16[256,512]{1,0:T(8,128)(2,1)S(1)}, bf16[256,512]{1,0:T(8,128)(2,1)S(1)}, u32[]{:S(2)}, u32[]{:S(2)}) collective-permute-start(bf16[256,512]{1,0:T(8,128)(2,1)S(1)} %bitcast.530), channel_id=1, source_target_pairs={{0,4},{1,5},{2,6},{3,7},{4,0},{5,1},{6,2},{7,3},{8,12},{9,13},{10,... | collective-permute-start | bytes 786440 | tf_op jit(solution)/shard_map/ppermute | solution.py:91
  360.4 11.8 %collective-permute-start.40 = (bf16[256,512]{1,0:T(8,128)(2,1)S(1)}, bf16[256,512]{1,0:T(8,128)(2,1)S(1)}, u32[]{:S(2)}, u32[]{:S(2)}) collective-permute-start(bf16[256,512]{1,0:T(8,128)(2,1)S(1)} %bitcast.528), channel_id=1, source_target_pairs={{0,2},{1,3},{2,0},{3,1},{4,6},{5,7},{6,4},{7,5},{8,10},{9,11},{10,... | collective-permute-start | bytes 786440 | tf_op jit(solution)/shard_map/ppermute | solution.py:91
  (40 other events, 314.3 us)
